TPU v7x, 32 devices: a whole 2x2x4 slice. The times are simulated.
32 devices in a mesh: grp: 2 (over y), dp: 2 (over x), kv: 4 (over z), tp: 2 (over core).
Axes of the slice: x: 2, y: 2, z: 4, core: 2. Of those that a mesh axis runs over, the one named last changes fastest.
Arguments:
- queries: bfloat16 [4, 1024, 2048], P(('grp', 'dp'), 'kv', 'tp'), parts along dimension 0, may hold values from -10 to 10
- keys: bfloat16 [4, 1024, 512], P(('grp', 'dp'), 'kv', 'tp'), parts along dimension 0, may hold values from -10 to 10
- values: bfloat16 [4, 1024, 512], P(('grp', 'dp'), 'kv', 'tp'), parts along dimension 0, may hold values from -6 to 6
- gate_logits: float32 [4, 2, 1024, 32], P(('grp', 'dp'), None, 'kv', 'tp'), parts along dimension 0, may hold values from -6 to 6
- chosen: int32 [4, 8, 8, 16], P(('grp', 'dp'), 'kv', 'tp'), parts along dimension 0, may hold values from -1 to 15, as said below
- pool_k: float32 [32, 64], replicated, may hold values from 0 to 0.35
- pool_v: float32 [32, 64], replicated, may hold values from 0 to 0.35
- out_gain: float32 [2048], P('tp'), may hold values from 0.1 to 1.9
Outputs:
- attended: bfloat16 [4, 1024, 2048], P(('grp', 'dp'), 'kv', 'tp'), parts along dimension 0
There are 2 independent parts, one for each index of `grp`. A program takes and returns all parts, laid end to end along the dimension named above; an argument that names none is the same for every part. Nothing has to cross between parts.
Inputs may be any that keep to these rules, and one draw needn't show every extreme that they name: Entries are key block numbers (block e holds positions e * 64 to e * 64 + 63) or -1 for none. The list of query block b (positions b * 128 onward) holds the blocks that contain its own positions, other distinct blocks that begin before it, and -1 in its remaining entries. For the query blocks of one span of 256 positions and one key head, the blocks chosen from any other span number at most 2; in every draw some span reaches 2.
All inputs are finite; a program needn't handle non-finite values.
Results may differ from a plain program's by a relative error of at most 0.0079.
Values may be sent and summed in bfloat16 or wider, within the bound.
A program may use at most 64 MiB of HBM per device.

v0:
```python
import jax
import jax.numpy as jnp
from jax import lax
from jax.sharding import PartitionSpec as P

DH = 64
CMP_STRIDE = 16
CMP_BLOCK = 32
SLC = 64
QB = 128
NSEL = 16
MOST = 2
THETA = 500000.0
EPS = 1e-06
NEG = -1e30


def shifted(block, axis, distance):
    devices = range(lax.axis_size(axis))
    route = [(i - distance, i) for i in devices if i - distance in devices]
    return lax.ppermute(block, axis, route)


def rotate(matrix, start, heads):
    length = matrix.shape[0]
    half = DH // 2
    place = (start + jnp.arange(length)).astype(jnp.float32)
    freq = jnp.power(jnp.float32(THETA), -(2.0 * jnp.arange(half).astype(jnp.float32)) / DH)
    angle = place[:, None] * freq[None, :]
    cosine = jnp.cos(angle)[:, None, :]
    sine = jnp.sin(angle)[:, None, :]
    parts = matrix.reshape(length, heads, DH).astype(jnp.float32)
    first = parts[..., :half]
    second = parts[..., half:]
    turned = jnp.concatenate([first * cosine - second * sine, second * cosine + first * sine], -1)
    return turned.reshape(length, heads * DH).astype(jnp.bfloat16)


def compress(extended, pool, groups):
    count = extended.shape[0] // CMP_STRIDE - 1
    parts = extended.reshape(count + 1, CMP_STRIDE, groups, DH).astype(jnp.float32)
    lower = jnp.einsum(
        "nigd,id->ngd", parts[:-1], pool[:CMP_STRIDE], precision=lax.Precision.HIGHEST
    )
    upper = jnp.einsum(
        "nigd,id->ngd", parts[1:], pool[CMP_STRIDE:], precision=lax.Precision.HIGHEST
    )
    return (lower + upper).astype(jnp.bfloat16)


def wanted_blocks(lists, owners, per_owner):
    groups = lists.shape[1]
    total = owners * per_owner
    hits = lists[..., None] == jnp.arange(total, dtype=jnp.int32)
    member = jnp.any(hits, axis=(0, 2)).astype(jnp.int32).reshape(groups, owners, per_owner)
    rank = jnp.cumsum(member, -1) - member
    slot_hit = (member[..., None] == 1) & (rank[..., None] == jnp.arange(MOST))
    local_ids = jnp.arange(per_owner, dtype=jnp.int32)[:, None]
    asked = jnp.sum(jnp.where(slot_hit, local_ids, 0), axis=2)
    return (asked.transpose(1, 0, 2), rank.reshape(groups, total))


def per_device(queries, keys, values, gate_logits, chosen, pool_k, pool_v, out_gain):
    queries = queries[0]
    keys = keys[0]
    values = values[0]
    logits = gate_logits[0]
    lists = chosen[0]
    length = queries.shape[0]
    groups = keys.shape[1] // DH
    heads = queries.shape[1] // DH
    per_group = heads // groups
    qblocks = length // QB
    owners = lax.axis_size("kv")
    myself = lax.axis_index("kv")
    start = myself * length
    scale = DH ** (-0.5)
    query_turned = rotate(queries, start, heads)
    key_turned = rotate(keys, start, groups)
    next_keys, next_values = shifted((keys[:CMP_STRIDE], values[:CMP_STRIDE]), "kv", -1)
    key_summary = compress(jnp.concatenate([keys, next_keys], 0), pool_k, groups)
    value_summary = compress(jnp.concatenate([values, next_values], 0), pool_v, groups)
    place = start + jnp.arange(length)
    query_group = queries.reshape(length, groups, per_group, DH).transpose(1, 2, 0, 3)
    part_keys = lax.all_gather(key_summary, "kv", axis=0, tiled=True)
    part_values = lax.all_gather(value_summary, "kv", axis=0, tiled=True)
    count = part_keys.shape[0]
    ends = jnp.arange(count) * CMP_STRIDE + CMP_BLOCK - 1
    allow = ends[None, :] <= place[:, None]

    def per_group_fold(item):
        query_part, key_part, value_part, top, total, summed = item
        score = (
            jnp.einsum("htd,nd->htn", query_part, key_part, preferred_element_type=jnp.float32)
            * scale
        )
        score = jnp.where(allow, score, NEG)
        fresh = jnp.maximum(top, jnp.max(score, -1))
        weight = jnp.where(allow, jnp.exp(score - fresh[..., None]), 0.0)
        shrink = jnp.exp(top - fresh)
        total = total * shrink + jnp.sum(weight, -1)
        summed = summed * shrink[..., None] + jnp.einsum(
            "htn,nd->htd",
            weight.astype(jnp.bfloat16),
            value_part,
            preferred_element_type=jnp.float32,
        )
        return (fresh, total, summed)

    top = jnp.full((groups, per_group, length), NEG, jnp.float32)
    total = jnp.zeros((groups, per_group, length), jnp.float32)
    summed = jnp.zeros((groups, per_group, length, DH), jnp.float32)
    top, total, summed = lax.map(
        per_group_fold,
        (
            query_group,
            part_keys.transpose(1, 0, 2),
            part_values.transpose(1, 0, 2),
            top,
            total,
            summed,
        ),
    )
    summary_out = summed / jnp.maximum(total, 1.0)[..., None]
    group_pick = jnp.arange(groups)[None, :, None]
    safe = jnp.maximum(lists, 0)
    per_owner = length // SLC
    asked_ids, rank = wanted_blocks(lists, owners, per_owner)
    requests = lax.all_to_all(asked_ids, "kv", split_axis=0, concat_axis=0, tiled=True)
    local_keys = key_turned.reshape(per_owner, SLC, groups, DH)
    local_values = values.reshape(per_owner, SLC, groups, DH)
    served = (local_keys[requests, :, group_pick, :], local_values[requests, :, group_pick, :])
    got_keys, got_values = (
        lax.all_to_all(served[0], "kv", split_axis=0, concat_axis=0, tiled=True),
        lax.all_to_all(served[1], "kv", split_axis=0, concat_axis=0, tiled=True),
    )

    def table(received, local):
        remote = received.transpose(1, 0, 2, 3, 4).reshape(groups, owners * MOST, SLC, DH)
        return jnp.concatenate([remote, local.transpose(2, 0, 1, 3)], 1)

    owner = safe // per_owner
    inner = safe % per_owner
    slot = jnp.where(owner == myself, owners * MOST + inner, owner * MOST + rank[group_pick, safe])
    key_sel = table(got_keys, local_keys)[group_pick, slot]
    value_sel = table(got_values, local_values)[group_pick, slot]
    query_blocks = query_turned.reshape(qblocks, QB, groups, per_group, DH)

    def attend(item):
        index, query_part, keys_part, values_part, picks = item
        place_q = start + index * QB + jnp.arange(QB)
        score = jnp.einsum(
            "tghd,gnkd->ghtnk", query_part, keys_part, preferred_element_type=jnp.float32
        )
        score = score.reshape(groups, per_group, QB, NSEL * SLC) * scale
        safe_picks = jnp.maximum(picks, 0)
        key_place = (safe_picks[..., None] * SLC + jnp.arange(SLC)).reshape(groups, NSEL * SLC)
        live = jnp.broadcast_to(picks[..., None] >= 0, (groups, NSEL, SLC)).reshape(
            groups, NSEL * SLC
        )
        allow = (live[:, None, :] & (key_place[:, None, :] <= place_q[None, :, None]))[:, None]
        score = jnp.where(allow, score, NEG)
        top_sel = jnp.max(score, -1, keepdims=True)
        weight = jnp.where(allow, jnp.exp(score - top_sel), 0.0)
        total_sel = jnp.sum(weight, -1)
        flat_values = values_part.reshape(groups, NSEL * SLC, DH)
        out = jnp.einsum(
            "ghtk,gkd->ghtd",
            weight.astype(jnp.bfloat16),
            flat_values,
            preferred_element_type=jnp.float32,
        )
        return out / total_sel[..., None]

    chosen_out = lax.map(attend, (jnp.arange(qblocks), query_blocks, key_sel, value_sel, lists))
    gates = jax.nn.sigmoid(logits)
    summary_rows = summary_out.transpose(2, 0, 1, 3).reshape(length, heads, DH)
    chosen_rows = chosen_out.transpose(0, 3, 1, 2, 4).reshape(length, heads, DH)
    mixed = gates[0][..., None] * summary_rows + gates[1][..., None] * chosen_rows
    normed = (
        mixed
        * lax.rsqrt(jnp.mean(mixed * mixed, -1, keepdims=True) + EPS)
        * out_gain.reshape(heads, DH)
    )
    return normed.reshape(1, length, heads * DH).astype(jnp.bfloat16)


def solution(mesh):
    in_specs = (
        P(("grp", "dp"), "kv", "tp"),
        P(("grp", "dp"), "kv", "tp"),
        P(("grp", "dp"), "kv", "tp"),
        P(("grp", "dp"), None, "kv", "tp"),
        P(("grp", "dp"), "kv", "tp", None),
        P(),
        P(),
        P("tp"),
    )
    out_specs = P(("grp", "dp"), "kv", "tp")
    return jax.shard_map(
        per_device, mesh=mesh, in_specs=in_specs, out_specs=out_specs, check_vma=False
    )
```

profile of v0, /device:TPU:0, one launch (start us, length us, event | category | flops | bytes accessed | tf_op | source)
XLA Modules:
  0.0 114.5 jit_solution(15482757723917872336)
XLA Ops:
  2.6 6.3 %all-to-all-start = ((s32[4,4,2]{1,2,0:T(2,128)}), s32[4,4,2]{1,2,0:T(2,128)S(1)}, u32[]{:S(2)}, u32[]{:S(2)}) async-start(s32[4,4,2]{1,2,0:T(2,128)} %copy.74), calls=%async_computation | async-start | bytes 8192 | tf_op jit(solution)/shard_map/all_to_all | solution.py:129
  9.6 1.3 %collective-permute-start.1 = (bf16[16,256]{1,0:T(8,128)(2,1)S(1)}, bf16[16,256]{1,0:T(8,128)(2,1)S(1)}, u32[]{:S(2)}, u32[]{:S(2)}) collective-permute-start(bf16[16,256]{1,0:T(8,128)(2,1)S(1)} %slice_bitcast_fusion.1), channel_id=1, source_target_pairs={{2,0},{4,2},{6,4},{3,1},{5,3},{7,5},{10,8},{12,10},{14,12},{11,9},... | collective-permute-start | bytes 24584 | tf_op jit(solution)/shard_map/ppermute | solution.py:21
  11.6 1.3 %collective-permute-start = (bf16[16,256]{1,0:T(8,128)(2,1)S(1)}, bf16[16,256]{1,0:T(8,128)(2,1)S(1)}, u32[]{:S(2)}, u32[]{:S(2)}) collective-permute-start(bf16[16,256]{1,0:T(8,128)(2,1)S(1)} %slice_bitcast_fusion.4), channel_id=1, source_target_pairs={{2,0},{4,2},{6,4},{3,1},{5,3},{7,5},{10,8},{12,10},{14,12},{11,9},... | collective-permute-start | bytes 24584 | tf_op jit(solution)/shard_map/ppermute | solution.py:21
  18.1 1.5 %gather_fusion.1 = s32[128]{0:T(128)S(1)} fusion(s32[4,16]{1,0:T(4,128)S(1)} %convert_subtract_fusion, s32[128]{0:T(128)S(1)} %reshape.454), kind=kCustom, calls=%fused_computation.1 | custom fusion | bytes 2048 | tf_op jit(solution)/shard_map/gather | solution.py:144
  26.7 1.1 reshape.513
  27.8 7.4 %all-to-all-start.2 = ((bf16[4,2,16384]{2,1,0:T(2,128)(2,1)}), bf16[4,2,16384]{2,1,0:T(2,128)(2,1)S(1)}, u32[]{:S(2)}, u32[]{:S(2)}) async-start(bf16[4,2,16384]{2,1,0:T(2,128)(2,1)} %reshape.513), calls=%async_computation.2 | async-start | bytes 524288 | tf_op jit(solution)/shard_map/all_to_all | solution.py:135
  35.9 1.1 reshape.511
  37.6 13.7 %all_gather.7 = bf16[64,4,64]{2,1,0:T(4,128)(2,1)S(1)} all-gather(bf16[16,4,64]{2,1,0:T(4,128)(2,1)S(1)} %fusion.39), channel_id=1, replica_groups=mesh['grp'=2,'dp'=2,'kv'=4,'tp'=2] {'kv'}, dimensions={0}, use_global_device_ids=true | all-gather | bytes 40960 | tf_op jit(solution)/shard_map/all_gather | solution.py:86
  51.6 13.3 %all_gather.6 = bf16[64,4,64]{2,0,1:T(8,128)(2,1)S(1)} all-gather(bf16[16,4,64]{2,0,1:T(8,128)(2,1)S(1)} %fusion.40), channel_id=1, replica_groups=mesh['grp'=2,'dp'=2,'kv'=4,'tp'=2] {'kv'}, dimensions={0}, use_global_device_ids=true | all-gather | bytes 40960 | tf_op jit(solution)/shard_map/all_gather | solution.py:85
  64.9 4.6 %all-to-all-start.1 = ((bf16[4,2,16384]{2,1,0:T(2,128)(2,1)}), bf16[4,2,16384]{2,1,0:T(2,128)(2,1)S(1)}, u32[]{:S(2)}, u32[]{:S(2)}) async-start(bf16[4,2,16384]{2,1,0:T(2,128)(2,1)} %reshape.511), calls=%async_computation.1 | async-start | bytes 524288 | tf_op jit(solution)/shard_map/all_to_all | solution.py:134
  69.5 5.2 %while.24 = (s32[]{:T(128)}, f32[4,4,256]{2,1,0:T(4,128)S(1)}, f32[4,4,256,64]{2,3,1,0:T(8,128)}, bf16[4,4,256,64]{2,3,1,0:T(8,128)(2,1)S(1)}, bf16[4,64,64]{2,1...) while((s32[]{:T(128)}, f32[4,4,256]{2,1,0:T(4,128)S(1)}, ...), condition=%wide.region_3.4_spmd.clone, body=%wide.region_0.3_spmd.clone.sunk | while | flops 17454080 | bytes 1326441 | solution.py:113
  75.1 1.2 %all-to-all-done.1 = bf16[4,2,16384]{2,1,0:T(2,128)(2,1)S(1)} async-done(((bf16[4,2,16384]{2,1,0:T(2,128)(2,1)}), bf16[4,2,16384]{2,1,0:T(2,128)(2,1)S(1)}, u32[]{:S(2)}, u32[]{:S(2)}) %all-to-all-start.1) | async-done | bytes 262176 | tf_op jit(solution)/shard_map/all_to_all | solution.py:134
  77.0 2.3 %gather_fusion.2 = bf16[128,64,64]{2,1,0:T(8,128)(2,1)} fusion(bf16[4,12,64,64]{3,2,1,0:T(8,128)(2,1)S(1)} %pad_maximum_fusion, s32[128]{0:T(128)S(1)} %reshape.460), kind=kCustom, calls=%fused_computation.2 | custom fusion | bytes 2098176 | tf_op jit(solution)/shard_map/gather | solution.py:145
  80.5 28.3 %while.23 = (s32[]{:T(128)}, f32[2,4,4,128,64]{3,4,2,1,0:T(8,128)}, s32[2,4,16]{2,1,0:T(4,128)S(1)}, s32[2]{0:T(128)S(1)}, s32[]{:T(128)}, /*index=5*/bf16[2,4,1...) while((s32[]{:T(128)}, f32[2,4,4,128,64]{3,4,2,1,0:T(8,128)}, ...), condition=%wide.region_10.11_spmd, body=%wide.region_7.10_spmd.sunk | while | flops 562172224 | bytes 65482908 | solution.py:175
  83.3 1.4 %compare_and_fusion.5 = pred[4,128,1024]{1,2,0:T(8,128)(4,1)S(1)} fusion(s32[128]{0:T(128)S(1)} %iota_add_fusion.5, s32[4,1024]{1,0:T(4,128)S(1)} %broadcast_add_fusion.2, pred[4,1024]{1,0:T(4,128)(4,1)S(1)} %and.110), kind=kLoop, calls=%fused_computation.15.clone.1 | loop fusion | flops 1048576 | bytes 545280 | tf_op jit(solution)/shard_map/while/body/eval_jaxpr/and | solution.py:161
  84.8 2.5 %select_reduce_fusion.5 = (f32[4,4,128]{2,1,0:T(4,128)S(1)}, f32[4,4,128,16,64]{2,4,1,3,0:T(8,128)S(1)}) fusion(pred[4,128,16,64]{1,3,2,0:T(8,128)(4,1)S(1)} %compare_and_fusion.4, bf16[2,128,4,4,64]{1,4,3,2,0:T(8,128)(2,1)} %get-tuple-element.346, s32[]{:T(128)S(6)} %copy.143, bf16[2,4,16,64,64]{4,3,2,1,0:T(8,128)(2,1)} %get-tuple-element.345), kind=kOutput, calls=%fused_computation.13.clone.1 | convolution fusion | flops 274724864 | bytes 10232832 | tf_op jit(solution)/shard_map/while/body/eval_jaxpr/tghd,gnkd->ghtnk/dot_general | solution.py:152
  87.3 2.1 %select_reduce_fusion.6 = f32[4,4,128]{2,1,0:T(4,128)S(1)} fusion(f32[4,4,128,16,64]{2,4,1,3,0:T(8,128)S(1)} %get-tuple-element.306, f32[4,4,128]{2,1,0:T(4,128)S(1)} %get-tuple-element.307, pred[4,128,16,64]{1,3,2,0:T(8,128)(4,1)S(1)} %compare_and_fusion.4), kind=kLoop, calls=%fused_computation.11.clone.1 | loop fusion | flops 8386560 | bytes 8929280 | tf_op jit(solution)/shard_map/while/body/eval_jaxpr/reduce_sum | solution.py:165
  90.3 2.4 %fusion.68 = bf16[4,4,128,1024]{2,3,1,0:T(8,128)(2,1)S(1)} fusion(f32[4,4,128,16,64]{2,4,3,1,0:T(8,128)S(1)} %copy.137, f32[4,4,128]{2,1,0:T(4,128)S(1)} %get-tuple-element.307, pred[4,128,1024]{1,2,0:T(8,128)(4,1)S(1)} %compare_and_fusion.5), kind=kLoop, calls=%fused_computation.10.clone.1 | loop fusion | flops 8388608 | bytes 13115392 | tf_op jit(solution)/shard_map/while/body/eval_jaxpr/convert_element_type | solution.py:169
  97.4 1.4 %compare_and_fusion.5 = pred[4,128,1024]{1,2,0:T(8,128)(4,1)S(1)} fusion(s32[128]{0:T(128)S(1)} %iota_add_fusion.5, s32[4,1024]{1,0:T(4,128)S(1)} %broadcast_add_fusion.2, pred[4,1024]{1,0:T(4,128)(4,1)S(1)} %and.110), kind=kLoop, calls=%fused_computation.15.clone.1 | loop fusion | flops 1048576 | bytes 545280 | tf_op jit(solution)/shard_map/while/body/eval_jaxpr/and | solution.py:161
  98.9 2.5 %select_reduce_fusion.5 = (f32[4,4,128]{2,1,0:T(4,128)S(1)}, f32[4,4,128,16,64]{2,4,1,3,0:T(8,128)S(1)}) fusion(pred[4,128,16,64]{1,3,2,0:T(8,128)(4,1)S(1)} %compare_and_fusion.4, bf16[2,128,4,4,64]{1,4,3,2,0:T(8,128)(2,1)} %get-tuple-element.346, s32[]{:T(128)S(6)} %copy.143, bf16[2,4,16,64,64]{4,3,2,1,0:T(8,128)(2,1)} %get-tuple-element.345), kind=kOutput, calls=%fused_computation.13.clone.1 | convolution fusion | flops 274724864 | bytes 10232832 | tf_op jit(solution)/shard_map/while/body/eval_jaxpr/tghd,gnkd->ghtnk/dot_general | solution.py:152
  101.4 2.1 %select_reduce_fusion.6 = f32[4,4,128]{2,1,0:T(4,128)S(1)} fusion(f32[4,4,128,16,64]{2,4,1,3,0:T(8,128)S(1)} %get-tuple-element.306, f32[4,4,128]{2,1,0:T(4,128)S(1)} %get-tuple-element.307, pred[4,128,16,64]{1,3,2,0:T(8,128)(4,1)S(1)} %compare_and_fusion.4), kind=kLoop, calls=%fused_computation.11.clone.1 | loop fusion | flops 8386560 | bytes 8929280 | tf_op jit(solution)/shard_map/while/body/eval_jaxpr/reduce_sum | solution.py:165
  104.4 2.4 %fusion.68 = bf16[4,4,128,1024]{2,3,1,0:T(8,128)(2,1)S(1)} fusion(f32[4,4,128,16,64]{2,4,3,1,0:T(8,128)S(1)} %copy.137, f32[4,4,128]{2,1,0:T(4,128)S(1)} %get-tuple-element.307, pred[4,128,1024]{1,2,0:T(8,128)(4,1)S(1)} %compare_and_fusion.5), kind=kLoop, calls=%fused_computation.10.clone.1 | loop fusion | flops 8388608 | bytes 13115392 | tf_op jit(solution)/shard_map/while/body/eval_jaxpr/convert_element_type | solution.py:169
  108.7 1.6 %fusion.33 = (f32[256,4,4]{0,2,1:T(4,128)S(1)}, f32[4,4,256,64]{2,3,1,0:T(8,128)S(1)}) fusion(f32[256,4,4]{0,2,1:T(4,128)S(1)} %mul.290, f32[256,4,4]{0,2,1:T(4,128)S(1)} %mul.287, f32[4,4,256,64]{2,3,1,0:T(8,128)S(1)} %copy-done.4, f32[4,4,256]{2,1,0:T(4,128)S(1)} %broadcast_maximum_fusion.1, f32[2,4,4,128,64]{3,4,2,1,0:T(8,128)} %get-tuple-element.87), kind=kLoop, calls=%fused_computation.57 | loop fusion | flops 1568768 | bytes 3211264 | tf_op jit(solution)/shard_map/reduce_sum | solution.py:182
  110.3 2.0 %copy.86 = f32[2,128,4,4,64]{1,0,4,3,2:T(2,128)S(1)} copy(f32[2,128,4,4,64]{1,4,3,2,0:T(8,128)} %bitcast.233) | data formatting | bytes 2097152 | tf_op jit(solution)/shard_map/transpose | solution.py:178
  (160 shorter events, 36.7 us)
Async XLA Ops:
  0.0 23.6 %copy-start.5 = (bf16[1,256,1024]{2,1,0:T(8,128)(2,1)S(1)}, bf16[1,256,1024]{2,1,0:T(8,128)(2,1)}, u32[]{:S(2)}) copy-start(bf16[1,256,1024]{2,1,0:T(8,128)(2,1)} %param.12) | copy-start | bytes 1572868
  2.6 23.2 %all-to-all-start = ((s32[4,4,2]{1,2,0:T(2,128)}), s32[4,4,2]{1,2,0:T(2,128)S(1)}, u32[]{:S(2)}, u32[]{:S(2)}) async-start(s32[4,4,2]{1,2,0:T(2,128)} %copy.74), calls=%async_computation | async-start | bytes 8192 | tf_op jit(solution)/shard_map/all_to_all | solution.py:129
  9.6 27.4 %collective-permute-start.1 = (bf16[16,256]{1,0:T(8,128)(2,1)S(1)}, bf16[16,256]{1,0:T(8,128)(2,1)S(1)}, u32[]{:S(2)}, u32[]{:S(2)}) collective-permute-start(bf16[16,256]{1,0:T(8,128)(2,1)S(1)} %slice_bitcast_fusion.1), channel_id=1, source_target_pairs={{2,0},{4,2},{6,4},{3,1},{5,3},{7,5},{10,8},{12,10},{14,12},{11,9},... | collective-permute-start | bytes 24584 | tf_op jit(solution)/shard_map/ppermute | solution.py:21
  11.6 25.8 %collective-permute-start = (bf16[16,256]{1,0:T(8,128)(2,1)S(1)}, bf16[16,256]{1,0:T(8,128)(2,1)S(1)}, u32[]{:S(2)}, u32[]{:S(2)}) collective-permute-start(bf16[16,256]{1,0:T(8,128)(2,1)S(1)} %slice_bitcast_fusion.4), channel_id=1, source_target_pairs={{2,0},{4,2},{6,4},{3,1},{5,3},{7,5},{10,8},{12,10},{14,12},{11,9},... | collective-permute-start | bytes 24584 | tf_op jit(solution)/shard_map/ppermute | solution.py:21
  19.6 17.4 %copy-start.2 = (bf16[1,256,256]{2,1,0:T(8,128)(2,1)S(1)}, bf16[1,256,256]{2,1,0:T(8,128)(2,1)}, u32[]{:S(2)}) copy-start(bf16[1,256,256]{2,1,0:T(8,128)(2,1)} %param.14) | copy-start | bytes 393220
  22.8 14.6 %copy-start.3 = (bf16[1,256,256]{2,1,0:T(8,128)(2,1)S(1)}, bf16[1,256,256]{2,1,0:T(8,128)(2,1)}, u32[]{:S(2)}) copy-start(bf16[1,256,256]{2,1,0:T(8,128)(2,1)} %param.13) | copy-start | bytes 393220
  27.8 37.1 %all-to-all-start.2 = ((bf16[4,2,16384]{2,1,0:T(2,128)(2,1)}), bf16[4,2,16384]{2,1,0:T(2,128)(2,1)S(1)}, u32[]{:S(2)}, u32[]{:S(2)}) async-start(bf16[4,2,16384]{2,1,0:T(2,128)(2,1)} %reshape.513), calls=%async_computation.2 | async-start | bytes 524288 | tf_op jit(solution)/shard_map/all_to_all | solution.py:135
  64.9 11.4 %all-to-all-start.1 = ((bf16[4,2,16384]{2,1,0:T(2,128)(2,1)}), bf16[4,2,16384]{2,1,0:T(2,128)(2,1)S(1)}, u32[]{:S(2)}, u32[]{:S(2)}) async-start(bf16[4,2,16384]{2,1,0:T(2,128)(2,1)} %reshape.511), calls=%async_computation.1 | async-start | bytes 524288 | tf_op jit(solution)/shard_map/all_to_all | solution.py:134
  74.7 5.7 %copy-start.6 = (s32[1,2,4,16]{3,2,1,0:T(4,128)S(1)}, s32[1,2,4,16]{3,2,1,0:T(4,128)}, u32[]{:S(2)}) copy-start(s32[1,2,4,16]{3,2,1,0:T(4,128)} %param.16) | copy-start | bytes 1540
  80.4 28.3 %copy-start.4 = (f32[4,4,256,64]{2,3,1,0:T(8,128)S(1)}, f32[4,4,256,64]{2,3,1,0:T(8,128)}, u32[]{:S(2)}) copy-start(f32[4,4,256,64]{2,3,1,0:T(8,128)} %get-tuple-element.85) | copy-start | bytes 3145732
  80.4 32.8 %copy-start.7 = (f32[1024]{0:T(1024)S(1)}, f32[1024]{0:T(1024)}, u32[]{:S(2)}) copy-start(f32[1024]{0:T(1024)} %param.19) | copy-start | bytes 12292
  90.3 2.4 %copy-start = (f32[2,4,4,128,64]{3,4,2,1,0:T(8,128)S(1)}, f32[2,4,4,128,64]{3,4,2,1,0:T(8,128)}, u32[]{:S(2)}) copy-start(f32[2,4,4,128,64]{3,4,2,1,0:T(8,128)} %get-tuple-element.331) | copy-start | bytes 3145732 | tf_op jit(solution)/shard_map/while
  93.6 1.0 copy-start.1
  104.4 2.4 %copy-start = (f32[2,4,4,128,64]{3,4,2,1,0:T(8,128)S(1)}, f32[2,4,4,128,64]{3,4,2,1,0:T(8,128)}, u32[]{:S(2)}) copy-start(f32[2,4,4,128,64]{3,4,2,1,0:T(8,128)} %get-tuple-element.331) | copy-start | bytes 3145732 | tf_op jit(solution)/shard_map/while
  107.7 1.0 copy-start.1
where the time goes:
time: 115 us; the launch traced here: 114 us
  local copies, waits for them, and re-layouts  29.9 us (26%)
  blocking collectives  27 us (23%)
  other arithmetic  22.1 us (19%)
  starting transfers between devices  21 us (18%)
  matrix products  11.2 us (10%)
  loops' own time  1.71 us (1%)
  waiting for transfers between devices  1.22 us (1%)
    all_gather x1, blocking collectives, per_device(): part_values = lax.all_gather(value_summary, 'kv', axis=0, tiled=True)  13.7 us
    all_gather x1, blocking collectives, per_device(): part_keys = lax.all_gather(key_summary, 'kv', axis=0, tiled=True)  13.3 us
    all_to_all x1, starting transfers between devices, per_device(): lax.all_to_all(served[1], 'kv', split_axis=0, concat_axis=0, tiled=True)  7.44 us
    all_to_all x1, starting transfers between devices, per_device(): lax.all_to_all(asked_ids, 'kv', split_axis=0, concat_axis=0, tiled=True)  6.35 us
    unnamed x21, local copies, waits for them, and re-layouts  5.66 us
    dot_general x2, matrix products, attend(): jnp.einsum('tghd,gnkd->ghtnk', query_part, keys_part, preferred_element_t...  5.03 us
    convert_element_type x2, other arithmetic, attend(): weight.astype(jnp.bfloat16)  4.81 us
    and x4, other arithmetic, attend(): live[:, None, :] & (key_place[:, None, :] <= place_q[None, :, None])  4.65 us
  transfers between devices with their start and end apart: 5, of which 1 were waited for; matrix products, arithmetic and copies ran while one was open for 21% of the time, Pallas kernels for 0%

commit v1 on v0

--- a/solution.py
+++ b/solution.py
@@ -13,6 +13,9 @@
 THETA = 500000.0
 EPS = 1e-06
 NEG = -1e30
+begin_blocks = lambda t0: jnp.concatenate(
+    lax.all_to_all(jnp.stack(lax.axis_size("kv") * [t0], 0), "kv", 0, 0), 0
+)
 
 
 def shifted(block, axis, distance):
@@ -82,7 +85,7 @@
     value_summary = compress(jnp.concatenate([values, next_values], 0), pool_v, groups)
     place = start + jnp.arange(length)
     query_group = queries.reshape(length, groups, per_group, DH).transpose(1, 2, 0, 3)
-    part_keys = lax.all_gather(key_summary, "kv", axis=0, tiled=True)
+    part_keys = begin_blocks(key_summary)
     part_values = lax.all_gather(value_summary, "kv", axis=0, tiled=True)
     count = part_keys.shape[0]
     ends = jnp.arange(count) * CMP_STRIDE + CMP_BLOCK - 1

time: 115 us -> 108 us (0.939)
  blocking collectives: 27 us -> 14.4 us
  starting transfers between devices: 21 us -> 23.5 us
  waiting for transfers between devices: 1.22 us -> 3.09 us
    all_gather x1 -> x0, blocking collectives: 13.3 us -> none  [per_device(): part_keys = lax.all_gather(key_summary, 'kv', axis=0, tiled=True)]
    all_to_all x0 -> x1, starting transfers between devices: none -> 7.44 us  [lax.all_to_all(jnp.stack(lax.axis_size('kv') * [t0], 0), 'kv', 0, 0)]
    all_to_all x1, starting transfers between devices: 7.44 us -> 3.4 us  [per_device(): lax.all_to_all(served[1], 'kv', split_axis=0, concat_axis=0, tiled=True)]
    all_to_all x0 -> x1, waiting for transfers between devices: none -> 1.87 us  [lax.all_to_all(jnp.stack(lax.axis_size('kv') * [t0], 0), 'kv', 0, 0)]
    unnamed x21 -> x24, local copies, waits for them, and re-layouts: 5.66 us -> 6.52 us
  transfers between devices with their start and end apart: 5 -> 6, of which waited for: 1 -> 2; matrix products, arithmetic and copies ran while one was open for 21% -> 23% of each run, Pallas kernels for 0% -> 0%
where the time goes in v1:
time: 108 us; the launch traced here: 107 us
  local copies, waits for them, and re-layouts  30.8 us (29%)
  starting transfers between devices  23.5 us (22%)
  other arithmetic  22.1 us (20%)
  blocking collectives  14.4 us (13%)
  matrix products  11.2 us (10%)
  waiting for transfers between devices  3.09 us (3%)
  loops' own time  1.71 us (2%)
    all_gather x1, blocking collectives, per_device(): part_values = lax.all_gather(value_summary, 'kv', axis=0, tiled=True)  14.4 us
    all_to_all x1, starting transfers between devices, lax.all_to_all(jnp.stack(lax.axis_size('kv') * [t0], 0), 'kv', 0, 0)  7.44 us
    unnamed x24, local copies, waits for them, and re-layouts  6.52 us
    all_to_all x1, starting transfers between devices, per_device(): lax.all_to_all(asked_ids, 'kv', split_axis=0, concat_axis=0, tiled=True)  6.35 us
    dot_general x2, matrix products, attend(): jnp.einsum('tghd,gnkd->ghtnk', query_part, keys_part, preferred_element_t...  5.02 us
    convert_element_type x2, other arithmetic, attend(): weight.astype(jnp.bfloat16)  4.79 us
    and x4, other arithmetic, attend(): live[:, None, :] & (key_place[:, None, :] <= place_q[None, :, None])  4.65 us
    reduce_sum x2, other arithmetic, attend(): total_sel = jnp.sum(weight, -1)  4.23 us
  transfers between devices with their start and end apart: 6, of which 2 were waited for; matrix products, arithmetic and copies ran while one was open for 23% of the time, Pallas kernels for 0%

profile of v1, /device:TPU:0, one launch (start us, length us, event | category | flops | bytes accessed | tf_op | source)
XLA Modules:
  0.0 107.3 jit_solution(8930825560568782811)
XLA Ops:
  2.6 6.3 %all-to-all-start.1 = ((s32[4,4,2]{1,2,0:T(2,128)}), s32[4,4,2]{1,2,0:T(2,128)S(1)}, u32[]{:S(2)}, u32[]{:S(2)}) async-start(s32[4,4,2]{1,2,0:T(2,128)} %copy.95), calls=%async_computation.1 | async-start | bytes 8192 | tf_op jit(solution)/shard_map/all_to_all | solution.py:132
  9.6 1.3 %collective-permute-start.1 = (bf16[16,256]{1,0:T(8,128)(2,1)S(1)}, bf16[16,256]{1,0:T(8,128)(2,1)S(1)}, u32[]{:S(2)}, u32[]{:S(2)}) collective-permute-start(bf16[16,256]{1,0:T(8,128)(2,1)S(1)} %slice_bitcast_fusion.1), channel_id=1, source_target_pairs={{2,0},{4,2},{6,4},{3,1},{5,3},{7,5},{10,8},{12,10},{14,12},{11,9},... | collective-permute-start | bytes 24584 | tf_op jit(solution)/shard_map/ppermute | solution.py:24
  11.6 1.3 %collective-permute-start = (bf16[16,256]{1,0:T(8,128)(2,1)S(1)}, bf16[16,256]{1,0:T(8,128)(2,1)S(1)}, u32[]{:S(2)}, u32[]{:S(2)}) collective-permute-start(bf16[16,256]{1,0:T(8,128)(2,1)S(1)} %slice_bitcast_fusion.4), channel_id=1, source_target_pairs={{2,0},{4,2},{6,4},{3,1},{5,3},{7,5},{10,8},{12,10},{14,12},{11,9},... | collective-permute-start | bytes 24584 | tf_op jit(solution)/shard_map/ppermute | solution.py:24
  16.9 1.1 %slice.72 = bf16[16,16,4,64]{3,2,1,0:T(4,128)(2,1)S(1)} reshape(bf16[1,256,256]{2,1,0:T(8,128)(2,1)} %param.14) | data formatting | bytes 262144 | tf_op jit(solution)/shard_map/slice | solution.py:46
  18.2 1.5 %gather_fusion.1 = s32[128]{0:T(128)S(1)} fusion(s32[4,16]{1,0:T(4,128)S(1)} %convert_subtract_fusion, s32[128]{0:T(128)S(1)} %reshape.460), kind=kCustom, calls=%fused_computation.1 | custom fusion | bytes 2048 | tf_op jit(solution)/shard_map/gather | solution.py:147
  27.0 7.4 %all-to-all-start = ((bf16[4,2,2048]{2,1,0:T(2,128)(2,1)}), bf16[4,2,2048]{2,1,0:T(2,128)(2,1)S(1)}, u32[]{:S(2)}, u32[]{:S(2)}) async-start(bf16[4,2,2048]{2,1,0:T(2,128)(2,1)} %reshape.521), calls=%async_computation | async-start | bytes 65536 | tf_op jit(solution)/shard_map/all_to_all | solution.py:17
  38.2 1.9 %all-to-all-done = bf16[4,2,2048]{2,1,0:T(2,128)(2,1)S(1)} async-done(((bf16[4,2,2048]{2,1,0:T(2,128)(2,1)}), bf16[4,2,2048]{2,1,0:T(2,128)(2,1)S(1)}, u32[]{:S(2)}, u32[]{:S(2)}) %all-to-all-start) | async-done | bytes 32800 | tf_op jit(solution)/shard_map/all_to_all | solution.py:17
  40.1 3.4 %all-to-all-start.3 = ((bf16[4,2,16384]{2,1,0:T(2,128)(2,1)}), bf16[4,2,16384]{2,1,0:T(2,128)(2,1)S(1)}, u32[]{:S(2)}, u32[]{:S(2)}) async-start(bf16[4,2,16384]{2,1,0:T(2,128)(2,1)} %reshape.519), calls=%async_computation.3 | async-start | bytes 524288 | tf_op jit(solution)/shard_map/all_to_all | solution.py:138
  43.9 14.4 %all_gather.3 = bf16[64,4,64]{2,1,0:T(4,128)(2,1)S(1)} all-gather(bf16[16,4,64]{2,1,0:T(4,128)(2,1)S(1)} %fusion.39), channel_id=1, replica_groups=mesh['grp'=2,'dp'=2,'kv'=4,'tp'=2] {'kv'}, dimensions={0}, use_global_device_ids=true | all-gather | bytes 40960 | tf_op jit(solution)/shard_map/all_gather | solution.py:89
  58.6 3.8 %all-to-all-start.2 = ((bf16[4,2,16384]{2,1,0:T(2,128)(2,1)}), bf16[4,2,16384]{2,1,0:T(2,128)(2,1)S(1)}, u32[]{:S(2)}, u32[]{:S(2)}) async-start(bf16[4,2,16384]{2,1,0:T(2,128)(2,1)} %reshape.517), calls=%async_computation.2 | async-start | bytes 524288 | tf_op jit(solution)/shard_map/all_to_all | solution.py:137
  62.4 5.2 %while.24 = (s32[]{:T(128)}, f32[4,4,256]{2,1,0:T(4,128)S(1)}, f32[4,4,256,64]{2,3,1,0:T(8,128)}, bf16[4,4,256,64]{2,3,1,0:T(8,128)(2,1)S(1)}, bf16[4,64,64]{2,1...) while((s32[]{:T(128)}, f32[4,4,256]{2,1,0:T(4,128)S(1)}, ...), condition=%wide.region_3.4_spmd.clone, body=%wide.region_0.3_spmd.clone.sunk | while | flops 17454080 | bytes 1326441 | solution.py:116
  67.9 1.2 %all-to-all-done.2 = bf16[4,2,16384]{2,1,0:T(2,128)(2,1)S(1)} async-done(((bf16[4,2,16384]{2,1,0:T(2,128)(2,1)}), bf16[4,2,16384]{2,1,0:T(2,128)(2,1)S(1)}, u32[]{:S(2)}, u32[]{:S(2)}) %all-to-all-start.2) | async-done | bytes 262176 | tf_op jit(solution)/shard_map/all_to_all | solution.py:137
  69.9 2.3 %gather_fusion.2 = bf16[128,64,64]{2,1,0:T(8,128)(2,1)} fusion(bf16[4,12,64,64]{3,2,1,0:T(8,128)(2,1)S(1)} %pad_maximum_fusion, s32[128]{0:T(128)S(1)} %reshape.466), kind=kCustom, calls=%fused_computation.2 | custom fusion | bytes 2098176 | tf_op jit(solution)/shard_map/gather | solution.py:148
  73.3 28.2 %while.23 = (s32[]{:T(128)}, f32[2,4,4,128,64]{3,4,2,1,0:T(8,128)}, s32[2,4,16]{2,1,0:T(4,128)S(1)}, s32[2]{0:T(128)S(1)}, s32[]{:T(128)}, /*index=5*/bf16[2,4,1...) while((s32[]{:T(128)}, f32[2,4,4,128,64]{3,4,2,1,0:T(8,128)}, ...), condition=%wide.region_10.11_spmd, body=%wide.region_7.10_spmd.sunk | while | flops 562172224 | bytes 65482908 | solution.py:178
  76.2 1.4 %compare_and_fusion.5 = pred[4,128,1024]{1,2,0:T(8,128)(4,1)S(1)} fusion(s32[128]{0:T(128)S(1)} %iota_add_fusion.5, s32[4,1024]{1,0:T(4,128)S(1)} %broadcast_add_fusion.2, pred[4,1024]{1,0:T(4,128)(4,1)S(1)} %and.110), kind=kLoop, calls=%fused_computation.15.clone.1 | loop fusion | flops 1048576 | bytes 545280 | tf_op jit(solution)/shard_map/while/body/eval_jaxpr/and | solution.py:164
  77.6 2.5 %select_reduce_fusion.5 = (f32[4,4,128]{2,1,0:T(4,128)S(1)}, f32[4,4,128,16,64]{2,4,1,3,0:T(8,128)S(1)}) fusion(pred[4,128,16,64]{1,3,2,0:T(8,128)(4,1)S(1)} %compare_and_fusion.4, bf16[2,128,4,4,64]{1,4,3,2,0:T(8,128)(2,1)} %get-tuple-element.362, s32[]{:T(128)S(6)} %copy.164, bf16[2,4,16,64,64]{4,3,2,1,0:T(8,128)(2,1)} %get-tuple-element.361), kind=kOutput, calls=%fused_computation.13.clone.1 | convolution fusion | flops 274724864 | bytes 10232832 | tf_op jit(solution)/shard_map/while/body/eval_jaxpr/tghd,gnkd->ghtnk/dot_general | solution.py:155
  80.2 2.1 %select_reduce_fusion.6 = f32[4,4,128]{2,1,0:T(4,128)S(1)} fusion(f32[4,4,128,16,64]{2,4,1,3,0:T(8,128)S(1)} %get-tuple-element.322, f32[4,4,128]{2,1,0:T(4,128)S(1)} %get-tuple-element.323, pred[4,128,16,64]{1,3,2,0:T(8,128)(4,1)S(1)} %compare_and_fusion.4), kind=kLoop, calls=%fused_computation.11.clone.1 | loop fusion | flops 8386560 | bytes 8929280 | tf_op jit(solution)/shard_map/while/body/eval_jaxpr/reduce_sum | solution.py:168
  83.1 2.4 %fusion.68 = bf16[4,4,128,1024]{2,3,1,0:T(8,128)(2,1)S(1)} fusion(f32[4,4,128,16,64]{2,4,3,1,0:T(8,128)S(1)} %copy.158, f32[4,4,128]{2,1,0:T(4,128)S(1)} %get-tuple-element.323, pred[4,128,1024]{1,2,0:T(8,128)(4,1)S(1)} %compare_and_fusion.5), kind=kLoop, calls=%fused_computation.10.clone.1 | loop fusion | flops 8388608 | bytes 13115392 | tf_op jit(solution)/shard_map/while/body/eval_jaxpr/convert_element_type | solution.py:172
  90.3 1.4 %compare_and_fusion.5 = pred[4,128,1024]{1,2,0:T(8,128)(4,1)S(1)} fusion(s32[128]{0:T(128)S(1)} %iota_add_fusion.5, s32[4,1024]{1,0:T(4,128)S(1)} %broadcast_add_fusion.2, pred[4,1024]{1,0:T(4,128)(4,1)S(1)} %and.110), kind=kLoop, calls=%fused_computation.15.clone.1 | loop fusion | flops 1048576 | bytes 545280 | tf_op jit(solution)/shard_map/while/body/eval_jaxpr/and | solution.py:164
  91.8 2.5 %select_reduce_fusion.5 = (f32[4,4,128]{2,1,0:T(4,128)S(1)}, f32[4,4,128,16,64]{2,4,1,3,0:T(8,128)S(1)}) fusion(pred[4,128,16,64]{1,3,2,0:T(8,128)(4,1)S(1)} %compare_and_fusion.4, bf16[2,128,4,4,64]{1,4,3,2,0:T(8,128)(2,1)} %get-tuple-element.362, s32[]{:T(128)S(6)} %copy.164, bf16[2,4,16,64,64]{4,3,2,1,0:T(8,128)(2,1)} %get-tuple-element.361), kind=kOutput, calls=%fused_computation.13.clone.1 | convolution fusion | flops 274724864 | bytes 10232832 | tf_op jit(solution)/shard_map/while/body/eval_jaxpr/tghd,gnkd->ghtnk/dot_general | solution.py:155
  94.3 2.1 %select_reduce_fusion.6 = f32[4,4,128]{2,1,0:T(4,128)S(1)} fusion(f32[4,4,128,16,64]{2,4,1,3,0:T(8,128)S(1)} %get-tuple-element.322, f32[4,4,128]{2,1,0:T(4,128)S(1)} %get-tuple-element.323, pred[4,128,16,64]{1,3,2,0:T(8,128)(4,1)S(1)} %compare_and_fusion.4), kind=kLoop, calls=%fused_computation.11.clone.1 | loop fusion | flops 8386560 | bytes 8929280 | tf_op jit(solution)/shard_map/while/body/eval_jaxpr/reduce_sum | solution.py:168
  97.3 2.4 %fusion.68 = bf16[4,4,128,1024]{2,3,1,0:T(8,128)(2,1)S(1)} fusion(f32[4,4,128,16,64]{2,4,3,1,0:T(8,128)S(1)} %copy.158, f32[4,4,128]{2,1,0:T(4,128)S(1)} %get-tuple-element.323, pred[4,128,1024]{1,2,0:T(8,128)(4,1)S(1)} %compare_and_fusion.5), kind=kLoop, calls=%fused_computation.10.clone.1 | loop fusion | flops 8388608 | bytes 13115392 | tf_op jit(solution)/shard_map/while/body/eval_jaxpr/convert_element_type | solution.py:172
  101.5 1.5 %fusion.33 = (f32[256,4,4]{0,2,1:T(4,128)S(1)}, f32[4,4,256,64]{2,3,1,0:T(8,128)S(1)}) fusion(f32[256,4,4]{0,2,1:T(4,128)S(1)} %mul.290, f32[256,4,4]{0,2,1:T(4,128)S(1)} %mul.287, f32[4,4,256,64]{2,3,1,0:T(8,128)S(1)} %copy-done.4, f32[4,4,256]{2,1,0:T(4,128)S(1)} %broadcast_maximum_fusion.1, f32[2,4,4,128,64]{3,4,2,1,0:T(8,128)} %get-tuple-element.87), kind=kLoop, calls=%fused_computation.57 | loop fusion | flops 1568768 | bytes 3211264 | tf_op jit(solution)/shard_map/reduce_sum | solution.py:185
  103.1 2.0 %copy.107 = f32[2,128,4,4,64]{1,0,4,3,2:T(2,128)S(1)} copy(f32[2,128,4,4,64]{1,4,3,2,0:T(8,128)} %bitcast.238) | data formatting | bytes 2097152 | tf_op jit(solution)/shard_map/transpose | solution.py:181
  (165 shorter events, 38.6 us)
Async XLA Ops:
  0.0 23.6 %copy-start.5 = (bf16[1,256,1024]{2,1,0:T(8,128)(2,1)S(1)}, bf16[1,256,1024]{2,1,0:T(8,128)(2,1)}, u32[]{:S(2)}) copy-start(bf16[1,256,1024]{2,1,0:T(8,128)(2,1)} %param.12) | copy-start | bytes 1572868
  2.6 23.2 %all-to-all-start.1 = ((s32[4,4,2]{1,2,0:T(2,128)}), s32[4,4,2]{1,2,0:T(2,128)S(1)}, u32[]{:S(2)}, u32[]{:S(2)}) async-start(s32[4,4,2]{1,2,0:T(2,128)} %copy.95), calls=%async_computation.1 | async-start | bytes 8192 | tf_op jit(solution)/shard_map/all_to_all | solution.py:132
  9.6 33.9 %collective-permute-start.1 = (bf16[16,256]{1,0:T(8,128)(2,1)S(1)}, bf16[16,256]{1,0:T(8,128)(2,1)S(1)}, u32[]{:S(2)}, u32[]{:S(2)}) collective-permute-start(bf16[16,256]{1,0:T(8,128)(2,1)S(1)} %slice_bitcast_fusion.1), channel_id=1, source_target_pairs={{2,0},{4,2},{6,4},{3,1},{5,3},{7,5},{10,8},{12,10},{14,12},{11,9},... | collective-permute-start | bytes 24584 | tf_op jit(solution)/shard_map/ppermute | solution.py:24
  11.6 14.2 %collective-permute-start = (bf16[16,256]{1,0:T(8,128)(2,1)S(1)}, bf16[16,256]{1,0:T(8,128)(2,1)S(1)}, u32[]{:S(2)}, u32[]{:S(2)}) collective-permute-start(bf16[16,256]{1,0:T(8,128)(2,1)S(1)} %slice_bitcast_fusion.4), channel_id=1, source_target_pairs={{2,0},{4,2},{6,4},{3,1},{5,3},{7,5},{10,8},{12,10},{14,12},{11,9},... | collective-permute-start | bytes 24584 | tf_op jit(solution)/shard_map/ppermute | solution.py:24
  16.9 8.9 %copy-start.3 = (bf16[1,256,256]{2,1,0:T(8,128)(2,1)S(1)}, bf16[1,256,256]{2,1,0:T(8,128)(2,1)}, u32[]{:S(2)}) copy-start(bf16[1,256,256]{2,1,0:T(8,128)(2,1)} %param.13) | copy-start | bytes 393220
  23.1 20.4 %copy-start.2 = (bf16[1,256,256]{2,1,0:T(8,128)(2,1)S(1)}, bf16[1,256,256]{2,1,0:T(8,128)(2,1)}, u32[]{:S(2)}) copy-start(bf16[1,256,256]{2,1,0:T(8,128)(2,1)} %param.14) | copy-start | bytes 393220
  27.0 13.1 %all-to-all-start = ((bf16[4,2,2048]{2,1,0:T(2,128)(2,1)}), bf16[4,2,2048]{2,1,0:T(2,128)(2,1)S(1)}, u32[]{:S(2)}, u32[]{:S(2)}) async-start(bf16[4,2,2048]{2,1,0:T(2,128)(2,1)} %reshape.521), calls=%async_computation | async-start | bytes 65536 | tf_op jit(solution)/shard_map/all_to_all | solution.py:17
  40.1 18.5 %all-to-all-start.3 = ((bf16[4,2,16384]{2,1,0:T(2,128)(2,1)}), bf16[4,2,16384]{2,1,0:T(2,128)(2,1)S(1)}, u32[]{:S(2)}, u32[]{:S(2)}) async-start(bf16[4,2,16384]{2,1,0:T(2,128)(2,1)} %reshape.519), calls=%async_computation.3 | async-start | bytes 524288 | tf_op jit(solution)/shard_map/all_to_all | solution.py:138
  58.6 10.5 %all-to-all-start.2 = ((bf16[4,2,16384]{2,1,0:T(2,128)(2,1)}), bf16[4,2,16384]{2,1,0:T(2,128)(2,1)S(1)}, u32[]{:S(2)}, u32[]{:S(2)}) async-start(bf16[4,2,16384]{2,1,0:T(2,128)(2,1)} %reshape.517), calls=%async_computation.2 | async-start | bytes 524288 | tf_op jit(solution)/shard_map/all_to_all | solution.py:137
  67.5 5.7 %copy-start.6 = (s32[1,2,4,16]{3,2,1,0:T(4,128)S(1)}, s32[1,2,4,16]{3,2,1,0:T(4,128)}, u32[]{:S(2)}) copy-start(s32[1,2,4,16]{3,2,1,0:T(4,128)} %param.16) | copy-start | bytes 1540
  73.3 28.3 %copy-start.4 = (f32[4,4,256,64]{2,3,1,0:T(8,128)S(1)}, f32[4,4,256,64]{2,3,1,0:T(8,128)}, u32[]{:S(2)}) copy-start(f32[4,4,256,64]{2,3,1,0:T(8,128)} %get-tuple-element.85) | copy-start | bytes 3145732
  73.3 32.7 %copy-start.7 = (f32[1024]{0:T(1024)S(1)}, f32[1024]{0:T(1024)}, u32[]{:S(2)}) copy-start(f32[1024]{0:T(1024)} %param.19) | copy-start | bytes 12292
  83.1 2.4 %copy-start = (f32[2,4,4,128,64]{3,4,2,1,0:T(8,128)S(1)}, f32[2,4,4,128,64]{3,4,2,1,0:T(8,128)}, u32[]{:S(2)}) copy-start(f32[2,4,4,128,64]{3,4,2,1,0:T(8,128)} %get-tuple-element.347) | copy-start | bytes 3145732 | tf_op jit(solution)/shard_map/while
  86.4 1.0 copy-start.1
  97.3 2.4 %copy-start = (f32[2,4,4,128,64]{3,4,2,1,0:T(8,128)S(1)}, f32[2,4,4,128,64]{3,4,2,1,0:T(8,128)}, u32[]{:S(2)}) copy-start(f32[2,4,4,128,64]{3,4,2,1,0:T(8,128)} %get-tuple-element.347) | copy-start | bytes 3145732 | tf_op jit(solution)/shard_map/while
  100.6 1.0 copy-start.1
